TPU v7x, 32 devices: a whole 2x2x4 slice. The times are simulated.
32 devices in a mesh: sp: 8 (over z, y), tp: 4 (over x, core).
Axes of the slice: x: 2, y: 2, z: 4, core: 2. Of those that a mesh axis runs over, the one named last changes fastest.
Arguments:
- queries: bfloat16 [1536, 2048], P('sp', 'tp'), may hold values from -100 to 100
- keys: bfloat16 [1536, 512], P('sp'), may hold values from -8 to 8
- values: bfloat16 [1536, 512], P('sp'), may hold values from -6 to 6
- diff_scale: float32 [8], P('tp'), may hold values from 0.3 to 0.8
- head_gain: float32 [256], replicated, may hold values from 0.1 to 1.9
- w_out: bfloat16 [2048, 2048], P('tp'), may hold values from -0.125 to 0.125
- residual: bfloat16 [1536, 2048], P(('sp', 'tp')), may hold values from -6 to 6
- norm_gain: float32 [2048], replicated, may hold values from 0.1 to 1.9
- route_ids: int32 [1536, 2], P(('sp', 'tp')), may hold values from 0 to 7, all different within a row; in each aligned block of 48 rows (0 to 47, 48 to 95, ...) at most 18 rows name the same one
- route_weights: float32 [1536, 2], P(('sp', 'tp')), may hold values from 0.2 to 1
- w_gate: bfloat16 [8, 2048, 3072], P('sp', None, 'tp'), may hold values from -0.125 to 0.125
- w_up: bfloat16 [8, 2048, 3072], P('sp', None, 'tp'), may hold values from -0.125 to 0.125
- w_down: bfloat16 [8, 3072, 2048], P('sp', 'tp'), may hold values from -0.109375 to 0.109375
Outputs:
- layer_out: bfloat16 [1536, 2048], P(('sp', 'tp'))
Inputs may be any that keep to these rules, and one draw needn't show every extreme that they name: `route_ids`: in each aligned block of 48 rows (the rows of one device), no expert is named more than 18 times, a bound that some block reaches; a row names 2 different experts.
All inputs are finite; a program needn't handle non-finite values.
Results may differ from a plain program's by a relative error of at most 0.014.
Values may be sent and summed in bfloat16 or wider, within the bound.
A program may use at most 128 MiB of HBM per device.

v0:
```python
import math
import jax
import jax.numpy as jnp
from jax import lax
from jax.sharding import PartitionSpec as P

KV_HEADS = 2
EPS = 1e-06
LOWEST = -1e30


def swapped(value, axis, apart):
    mask = 2**apart
    pairs = [(source, source ^ mask) for source in range(lax.axis_size(axis))]
    return lax.ppermute(value, axis, pairs)


def attend(carry, piece, q_heads):
    half = q_heads.shape[-1]
    scale = 1.0 / math.sqrt(half)
    high, total, acc = carry
    rows = piece.shape[0]
    for first in range(0, rows, 2048):
        count = min(2048, rows - first)
        k_block = piece[first : first + count, : 2 * half].reshape(count, 2, half)
        v_block = piece[first : first + count, 2 * half :]
        scores = (
            jnp.einsum("qhmd,kmd->qhmk", q_heads, k_block, preferred_element_type=jnp.float32)
            * scale
        )
        peak = jnp.maximum(high, jnp.max(scores, axis=-1))
        fade = jnp.exp(high - peak)
        weights = jnp.exp(scores - peak[..., None]).astype(jnp.bfloat16)
        total = total * fade + jnp.sum(weights, axis=-1, dtype=jnp.float32)
        acc = acc * fade[..., None] + jnp.einsum(
            "qhmk,kd->qhmd", weights, v_block, preferred_element_type=jnp.float32
        )
        high = peak
    return (high, total, acc)


def local(
    queries,
    keys,
    values,
    diff_scale,
    head_gain,
    w_out,
    residual,
    norm_gain,
    route_ids,
    route_weights,
    w_gate,
    w_up,
    w_down,
):
    q_rows = queries.shape[0]
    heads_dev = diff_scale.shape[0]
    half_dim = queries.shape[1] // (2 * heads_dev)
    q_heads = queries.reshape(q_rows, heads_dev, 2, half_dim)
    group_cols = keys.shape[1] // KV_HEADS
    value_cols = values.shape[1] // KV_HEADS
    group = lax.axis_index("tp") // (lax.axis_size("tp") // KV_HEADS)
    k_group = lax.dynamic_slice_in_dim(keys, group * group_cols, group_cols, 1)
    v_group = lax.dynamic_slice_in_dim(values, group * value_cols, value_cols, 1)
    joined = jnp.concatenate([k_group, v_group], axis=1)
    start_state = (
        jnp.full((q_rows, heads_dev, 2), LOWEST, jnp.float32),
        jnp.zeros((q_rows, heads_dev, 2), jnp.float32),
        jnp.zeros((q_rows, heads_dev, 2, value_cols), jnp.float32),
    )
    part_rows = joined.shape[0] // 2
    side = lax.axis_index("tp") % 2
    own_half = lax.dynamic_slice_in_dim(joined, side * part_rows, part_rows, 0)
    near = lax.all_gather(own_half, "sp", axis=0, tiled=True)
    far = swapped(near, "tp", 0)
    high, total, acc = attend(attend(start_state, near, q_heads), far, q_heads)
    mixed = (
        acc[:, :, 0] / total[:, :, 0:1]
        - diff_scale[None, :, None] * acc[:, :, 1] / total[:, :, 1:2]
    )
    mixed = mixed * lax.rsqrt(jnp.mean(mixed * mixed, axis=-1, keepdims=True) + EPS) * head_gain
    head_out = mixed.astype(jnp.bfloat16).reshape(q_rows, heads_dev * value_cols)
    rows_out = residual.shape[0]
    attended = lax.psum_scatter(
        jnp.dot(head_out, w_out, preferred_element_type=jnp.float32).astype(jnp.bfloat16),
        "tp",
        scatter_dimension=0,
        tiled=True,
    ).astype(jnp.float32)
    state = residual.astype(jnp.float32) + attended
    normed = (
        state * lax.rsqrt(jnp.mean(state * state, axis=-1, keepdims=True) + EPS) * norm_gain
    ).astype(jnp.bfloat16)
    experts = lax.axis_size("sp")
    top = route_ids.shape[1]
    width = normed.shape[1]
    capacity = max(2, 3 * rows_out * top // (2 * experts))
    flat_ids = route_ids.reshape(-1)
    onehot = (flat_ids[:, None] == jnp.arange(experts, dtype=jnp.int32)[None, :]).astype(jnp.int32)
    slot = jnp.sum((jnp.cumsum(onehot, axis=0) - onehot) * onehot, axis=1)
    dest = flat_ids * capacity + slot
    copies = jnp.repeat(normed, top, axis=0)
    outgoing = (
        jnp.zeros((experts * capacity, width), jnp.bfloat16)
        .at[dest]
        .set(copies)
        .reshape(experts, capacity, width)
    )
    gathered = lax.all_gather(
        lax.all_to_all(outgoing, "sp", split_axis=0, concat_axis=0, tiled=True),
        "tp",
        axis=0,
        tiled=True,
    )
    flat = gathered.reshape(-1, width)
    gate = jnp.dot(flat, w_gate[0], preferred_element_type=jnp.float32)
    up = jnp.dot(flat, w_up[0], preferred_element_type=jnp.float32)
    hidden = (jax.nn.silu(gate) * up).astype(jnp.bfloat16)
    partial_value = jnp.dot(hidden, w_down[0], preferred_element_type=jnp.float32).reshape(
        gathered.shape[0], gathered.shape[1], width
    )
    served = lax.psum_scatter(
        partial_value.astype(jnp.bfloat16), "tp", scatter_dimension=0, tiled=True
    )
    returned = lax.all_to_all(served, "sp", split_axis=0, concat_axis=0, tiled=True).reshape(
        experts * capacity, width
    )
    picked = returned[dest].reshape(rows_out, top, width)
    expert_sum = jnp.einsum("rt,rtd->rd", route_weights, picked.astype(jnp.float32))
    return (state + expert_sum).astype(jnp.bfloat16)


def solution(mesh):
    in_specs = (
        P("sp", "tp"),
        P("sp", None),
        P("sp", None),
        P("tp"),
        P(),
        P("tp", None),
        P(("sp", "tp"), None),
        P(),
        P(("sp", "tp"), None),
        P(("sp", "tp"), None),
        P("sp", None, "tp"),
        P("sp", None, "tp"),
        P("sp", "tp", None),
    )
    out_specs = P(("sp", "tp"), None)
    return jax.shard_map(local, mesh=mesh, in_specs=in_specs, out_specs=out_specs, check_vma=False)
```

profile of v0, /device:TPU:0, one launch (start us, length us, event | category | flops | bytes accessed | tf_op | source)
XLA Modules:
  0.0 259.2 jit_solution(16398461399570761725)
XLA Ops:
  6.6 1.1 constant_dynamic-slice_fusion
  7.8 36.0 %all_gather.6 = bf16[768,512]{1,0:T(8,128)(2,1)} all-gather(bf16[96,512]{1,0:T(8,128)(2,1)S(1)} %fusion.36), channel_id=1, replica_groups=mesh['sp'=8,'tp'=4] {'sp'}, dimensions={0}, use_global_device_ids=true | all-gather | bytes 884736 | tf_op jit(solution)/shard_map/all_gather | solution.py:75
  43.8 1.8 slice.34
  45.6 1.9 copy.43
  48.2 2.9 %bitcast_reduce_fusion.1 = (f32[192,2,2]{0,1,2:T(2,128)S(1)}, f32[2,768,192,2]{1,2,3,0:T(8,128)}) fusion(bf16[768,2,128,1]{0,2,3,1:T(8,128)(2,1)} %bitcast.119, bf16[192,2,2,128]{3,2,1,0:T(2,128)(2,1)S(1)} %reshape.102), kind=kOutput, calls=%fused_computation.16 | convolution fusion | flops 152173824 | bytes 2952192 | tf_op jit(solution)/shard_map/qhmd,kmd->qhmk/dot_general | solution.py:28
  51.0 1.8 slice.36
  52.8 1.9 reshape.103
  54.6 1.6 bitcast_reduce_fusion
  56.9 1.0 copy-done.1
  58.6 1.5 fusion.18
  60.1 1.5 convolution_add_fusion
  61.6 0.9 copy-done.2
  62.4 0.8 slice_bitcast_fusion.4
  63.3 0.8 copy.77
  64.0 1.4 fusion.28
  65.5 0.8 copy.78
  66.2 1.3 copy.53
  67.5 0.8 copy.80
  68.6 0.8 copy.83
  69.9 1.3 div.58.clone
  71.2 1.2 div.62.clone
  72.5 2.6 %convolution_convert_fusion = bf16[192,2048]{1,0:T(8,128)(2,1)} fusion(bf16[512,2048]{1,0:T(8,128)(2,1)S(1)} %copy-done.15, f32[192,512]{1,0:T(8,128)S(1)} %bitcast.124, f32[192,512]{1,0:T(8,128)S(1)} %bitcast.126, f32[192,512]{1,0:T(8,128)S(1)} %bitcast.123, f32[192,512]{1,0:T(8,128)} %bitcast.122, f32[192,512]{1,0:T(8,128)S(1)} %bitcast.125, ...), kind=kOutput, calls=%fused_computation.10 | convolution fusion | flops 403734528 | bytes 4853760 | tf_op jit(solution)/shard_map/dot_general | solution.py:86
  76.0 23.4 %reduce-scatter.5.cloned.1.call-done = bf16[48,2048]{1,0:T(8,128)(2,1)} async-done(((bf16[192,2048]{1,0:T(8,128)(2,1)}), bf16[48,2048]{1,0:T(8,128)(2,1)}) %reduce-scatter.5.cloned.1.call-update) | async-done | bytes 196624 | tf_op jit(solution)/shard_map/reduce_scatter | solution.py:85
  99.4 1.1 multiply_reduce_fusion
  100.6 1.0 multiply_convert_fusion.1
  101.6 1.0 broadcast_in_dim.11
  102.6 1.9 reshape.121
  104.5 2.5 scatter_custom_fusion
  107.0 2.1 reshape.105
  109.1 25.5 %all_to_all.10 = bf16[8,18,2048]{2,1,0:T(8,128)(2,1)S(1)} all-to-all(bf16[8,18,2048]{2,1,0:T(8,128)(2,1)} %reshape.105), channel_id=1, replica_groups=mesh['sp'=8,'tp'=4] {'sp'}, dimensions={0} | all-to-all | bytes 1179648 | tf_op jit(solution)/shard_map/all_to_all | solution.py:111
  134.6 1.2 copy.60
  136.0 22.0 %all-gather.2.cloned.1.call-done = bf16[32,18,2048]{2,0,1:T(8,128)(2,1)} async-done(((bf16[8,18,2048]{2,0,1:T(8,128)(2,1)}), bf16[32,18,2048]{2,0,1:T(8,128)(2,1)}) %all-gather.2.cloned.1.call-update) | async-done | bytes 2359312 | tf_op jit(solution)/shard_map/all_gather | solution.py:110
  158.1 4.7 %copy.61 = bf16[32,18,2048]{2,1,0:T(8,128)(2,1)} copy(bf16[32,18,2048]{2,0,1:T(8,128)(2,1)} %all-gather.2.cloned.1.call-done) | data formatting | bytes 4718592 | tf_op jit(solution)/shard_map/all_gather | solution.py:110
  162.7 4.3 %reshape.106 = bf16[576,2048]{1,0:T(8,128)(2,1)} reshape(bf16[32,18,2048]{2,1,0:T(8,128)(2,1)} %copy.61) | data formatting | bytes 4718592 | tf_op jit(solution)/shard_map/reshape | solution.py:116
  167.1 4.7 %fusion.4 = f32[576,768]{1,0:T(8,128)S(1)} fusion(bf16[576,2048]{1,0:T(8,128)(2,1)} %reshape.106, bf16[1,2048,768]{2,1,0:T(8,128)(2,1)} %param.23), kind=kOutput, calls=%fused_computation.6 | convolution fusion | flops 1811939328 | bytes 7274496 | tf_op jit(solution)/shard_map/dot_general | solution.py:117
  171.8 3.1 %multiply_convert_fusion = bf16[576,768]{1,0:T(8,128)(2,1)} fusion(f32[576,768]{1,0:T(8,128)S(1)} %fusion.4, bf16[576,2048]{1,0:T(8,128)(2,1)S(1)} %copy-done.3, bf16[1,2048,768]{2,1,0:T(8,128)(2,1)S(1)} %copy-done.14), kind=kOutput, calls=%fused_computation.21 | convolution fusion | flops 1814593536 | bytes 8159232 | tf_op jit(solution)/shard_map/dot_general | solution.py:118
  174.9 2.2 dot_general.36
  177.1 3.3 %fusion.9 = bf16[18,4,8,2048]{3,2,1,0:T(8,128)(2,1)S(1)} fusion(bf16[1,768,2048]{2,1,0:T(8,128)(2,1)S(1)} %copy-done, bf16[32,18,768]{2,1,0:T(8,128)(2,1)} %dot_general.36), kind=kOutput, calls=%fused_computation.9 | convolution fusion | flops 1813118976 | bytes 6389760 | tf_op jit(solution)/shard_map/dot_general | solution.py:120
  180.4 1.6 copy.79
  182.0 33.0 %reduce-scatter.7.cloned.1.call-done = bf16[8,36864]{1,0:T(8,128)(2,1)} async-done(((bf16[32,36864]{1,0:T(8,128)(2,1)}), bf16[8,36864]{1,0:T(8,128)(2,1)}) %reduce-scatter.7.cloned.1.call-update) | async-done | bytes 589840
  215.0 2.3 copy.63
  217.3 5.5 %all-to-all-start.1 = ((bf16[8,18,2048]{2,1,0:T(8,128)(2,1)}), bf16[8,18,2048]{2,1,0:T(8,128)(2,1)}, u32[]{:S(2)}, u32[]{:S(2)}) async-start(bf16[8,18,2048]{2,1,0:T(8,128)(2,1)} %copy.63), calls=%async_computation.2 | async-start | bytes 1572864 | tf_op jit(solution)/shard_map/all_to_all | solution.py:126
  223.5 19.4 %all-to-all-done.1 = bf16[8,18,2048]{2,1,0:T(8,128)(2,1)} async-done(((bf16[8,18,2048]{2,1,0:T(8,128)(2,1)}), bf16[8,18,2048]{2,1,0:T(8,128)(2,1)}, u32[]{:S(2)}, u32[]{:S(2)}) %all-to-all-start.1) | async-done | bytes 589856 | tf_op jit(solution)/shard_map/all_to_all | solution.py:126
  243.0 2.1 reshape.107
  245.1 3.1 %gather_fusion = bf16[96,2048]{1,0:T(8,128)(2,1)} fusion(bf16[144,2048]{1,0:T(8,128)(2,1)} %reshape.107, s32[1024]{0:T(1024)S(1)} %pad_clamp_fusion), kind=kCustom, calls=%fused_computation | custom fusion | bytes 786816 | tf_op jit(solution)/shard_map/gather | solution.py:129
  248.2 2.0 reshape.108
  250.3 1.5 fusion.42
  251.8 0.8 fusion.24
  (70 shorter events, 4.8 us)
Async XLA Ops:
  6.5 170.6 %copy-start = (bf16[1,768,2048]{2,1,0:T(8,128)(2,1)S(1)}, bf16[1,768,2048]{2,1,0:T(8,128)(2,1)}, u32[]{:S(2)}) copy-start(bf16[1,768,2048]{2,1,0:T(8,128)(2,1)} %param.25) | copy-start | bytes 9437188
  6.5 39.0 %copy-start.7 = (bf16[192,512]{1,0:T(8,128)(2,1)S(1)}, bf16[192,512]{1,0:T(8,128)(2,1)}, u32[]{:S(2)}) copy-start(bf16[192,512]{1,0:T(8,128)(2,1)} %param.13) | copy-start | bytes 589828
  6.5 41.0 %copy-start.11 = (f32[2]{0:T(128)S(1)}, f32[2]{0:T(128)}, u32[]{:S(2)}) copy-start(f32[2]{0:T(128)} %param.16) | copy-start | bytes 28
  6.5 41.0 %copy-start.12 = (f32[256]{0:T(256)S(1)}, f32[256]{0:T(256)}, u32[]{:S(2)}) copy-start(f32[256]{0:T(256)} %param.17) | copy-start | bytes 3076
  6.5 92.9 %reduce-scatter.5.cloned.1.call-start = ((), (), s32[]{:S(2)}) async-start(), calls=%async_computation.4 | async-start | bytes 983040 | tf_op jit(solution)/shard_map/reduce_scatter | solution.py:85
  43.8 7.3 %collective-permute-start = (bf16[768,512]{1,0:T(8,128)(2,1)}, bf16[768,512]{1,0:T(8,128)(2,1)}, u32[]{:S(2)}, u32[]{:S(2)}) collective-permute-start(bf16[768,512]{1,0:T(8,128)(2,1)} %all_gather.6), channel_id=1, source_target_pairs={{0,1},{1,0},{2,3},{3,2},{4,5},{5,4},{6,7},{7,6},{8,9},{9,8},{10,11... | collective-permute-start | bytes 2359304 | tf_op jit(solution)/shard_map/ppermute | solution.py:15
  56.2 1.7 copy-start.1
  61.6 0.9 copy-start.2
  68.6 3.8 %copy-start.10 = (f32[1,2,2,128]{3,1,2,0:T(2,128)S(1)}, f32[1,2,2,128]{3,1,2,0:T(2,128)}, u32[]{:S(2)}) copy-start(f32[1,2,2,128]{3,1,2,0:T(2,128)} %copy.86) | copy-start | bytes 6148
  69.5 2.9 %copy-start.6 = (f32[24,8,2,256]{3,1,2,0:T(8,128)S(1)}, f32[24,8,2,256]{3,1,2,0:T(8,128)}, u32[]{:S(2)}) copy-start(f32[24,8,2,256]{3,1,2,0:T(8,128)} %copy.83) | copy-start | bytes 1179652
  69.5 2.9 %copy-start.15 = (bf16[512,2048]{1,0:T(8,128)(2,1)S(1)}, bf16[512,2048]{1,0:T(8,128)(2,1)}, u32[]{:S(2)}) copy-start(bf16[512,2048]{1,0:T(8,128)(2,1)} %param.18) | copy-start | bytes 6291460
  72.4 2.7 %copy-start.9 = (s32[48,2]{0,1:T(2,128)S(1)}, s32[48,2]{0,1:T(2,128)}, u32[]{:S(2)}) copy-start(s32[48,2]{0,1:T(2,128)} %param.21) | copy-start | bytes 1156
  72.5 27.0 %copy-start.4 = (bf16[48,2048]{1,0:T(8,128)(2,1)S(1)}, bf16[48,2048]{1,0:T(8,128)(2,1)}, u32[]{:S(2)}) copy-start(bf16[48,2048]{1,0:T(8,128)(2,1)} %param.19) | copy-start | bytes 589828
  72.5 28.1 %copy-start.8 = (f32[2048]{0:T(1024)S(1)}, f32[2048]{0:T(1024)}, u32[]{:S(2)}) copy-start(f32[2048]{0:T(1024)} %param.20) | copy-start | bytes 24580
  75.1 83.0 %all-gather.2.cloned.1.call-start = ((), (), s32[]{:S(2)}) async-start(), calls=%async_computation.5 | async-start | bytes 2949120 | tf_op jit(solution)/shard_map/all_gather | solution.py:110
  135.8 79.2 %reduce-scatter.7.cloned.1.call-start = ((), (), s32[]{:S(2)}) async-start(), calls=%async_computation.6 | async-start | bytes 2949120
  167.1 4.7 %copy-start.3 = (bf16[576,2048]{1,0:T(8,128)(2,1)S(1)}, bf16[576,2048]{1,0:T(8,128)(2,1)}, u32[]{:S(2)}) copy-start(bf16[576,2048]{1,0:T(8,128)(2,1)} %reshape.106) | copy-start | bytes 7077892
  167.1 4.8 %copy-start.14 = (bf16[1,2048,768]{2,1,0:T(8,128)(2,1)S(1)}, bf16[1,2048,768]{2,1,0:T(8,128)(2,1)}, u32[]{:S(2)}) copy-start(bf16[1,2048,768]{2,1,0:T(8,128)(2,1)} %param.24) | copy-start | bytes 9437188
  182.0 40.8 %copy-start.13 = (f32[48,2]{0,1:T(2,128)S(1)}, f32[48,2]{0,1:T(2,128)}, u32[]{:S(2)}) copy-start(f32[48,2]{0,1:T(2,128)} %param.22) | copy-start | bytes 1156
  217.3 25.7 %all-to-all-start.1 = ((bf16[8,18,2048]{2,1,0:T(8,128)(2,1)}), bf16[8,18,2048]{2,1,0:T(8,128)(2,1)}, u32[]{:S(2)}, u32[]{:S(2)}) async-start(bf16[8,18,2048]{2,1,0:T(8,128)(2,1)} %copy.63), calls=%async_computation.2 | async-start | bytes 1572864 | tf_op jit(solution)/shard_map/all_to_all | solution.py:126
  245.1 6.7 %copy-start.5 = (bf16[48,2048]{1,0:T(8,128)(2,1)S(1)}, bf16[48,2048]{1,0:T(8,128)(2,1)}, u32[]{:S(2)}) copy-start(bf16[48,2048]{1,0:T(8,128)(2,1)} %reduce-scatter.5.cloned.1.call-done) | copy-start | bytes 589828
Sparse Core Ops, SparseCore 0:
  75.2 24.1 reduce-scatter.4
  135.9 22.1 all-gather.1
  182.1 32.8 reduce-scatter.6
where the time goes:
time: 260 us; the launch traced here: 259 us
  waiting for transfers between devices  97.9 us (38%)
  blocking collectives  61.5 us (24%)
  local copies, waits for them, and re-layouts  51.7 us (20%)
  matrix products  22.6 us (9%)
  between operations  13.5 us (5%)
  other arithmetic  6.16 us (2%)
  starting transfers between devices  5.82 us (2%)
    all_gather x1, blocking collectives, local(): near = lax.all_gather(own_half, 'sp', axis=0, tiled=True)  36 us
    unnamed x4, waiting for transfers between devices  33 us
    all_to_all x1, blocking collectives, local(): lax.all_to_all(outgoing, 'sp', split_axis=0, concat_axis=0, tiled=True)  25.5 us
    reduce_scatter x1, waiting for transfers between devices, local(): lax.psum_scatter(jnp.dot(head_out, w_out, preferred_element_type=jnp.floa...  23.4 us
    all_gather x1, waiting for transfers between devices, local(): lax.all_gather(lax.all_to_all(outgoing, 'sp', split_axis=0, concat_axis=0...  22 us
    all_to_all x1, waiting for transfers between devices, local(): lax.all_to_all(served, 'sp', split_axis=0, concat_axis=0, tiled=True)  19.4 us
    unnamed x47, local copies, waits for them, and re-layouts  8.96 us
    all_to_all x1, starting transfers between devices, local(): lax.all_to_all(served, 'sp', split_axis=0, concat_axis=0, tiled=True)  5.52 us
  transfers between devices with their start and end apart: 5, of which 4 were waited for; matrix products, arithmetic and copies ran while one was open for 3% of the time, Pallas kernels for 0%

commit v1 on v0

--- a/solution.py
+++ b/solution.py
@@ -72,7 +72,12 @@
     part_rows = joined.shape[0] // 2
     side = lax.axis_index("tp") % 2
     own_half = lax.dynamic_slice_in_dim(joined, side * part_rows, part_rows, 0)
-    near = lax.all_gather(own_half, "sp", axis=0, tiled=True)
+    ring = [own_half]
+    for hop in range(7):
+        ring.append(lax.ppermute(ring[-1], "sp", [(dev, (dev + 1) % 8) for dev in range(8)]))
+    near = jnp.roll(
+        jnp.concatenate(ring[::-1], axis=0), (lax.axis_index("sp") + 1) * ring[0].shape[0], axis=0
+    )
     far = swapped(near, "tp", 0)
     high, total, acc = attend(attend(start_state, near, q_heads), far, q_heads)
     mixed = (

time: 260 us -> 284 us (1.092)
  waiting for transfers between devices: 97.9 us -> 144 us
  blocking collectives: 61.5 us -> 25.5 us
  local copies, waits for them, and re-layouts: 51.7 us -> 62.3 us
  starting transfers between devices: 5.82 us -> 8.85 us
    ppermute x0 -> x7, waiting for transfers between devices: none -> 50 us  [local(): lax.ppermute(ring[-1], 'sp', [(dev, (dev + 1) % 8) for dev in range(8)])]
    all_gather x1 -> x0, blocking collectives: 36 us -> none  [local(): near = lax.all_gather(own_half, 'sp', axis=0, tiled=True)]
    unnamed x47 -> x82, local copies, waits for them, and re-layouts: 8.96 us -> 19 us
    reduce_scatter x1, waiting for transfers between devices: 23.4 us -> 20 us  [local(): lax.psum_scatter(jnp.dot(head_out, w_out, preferred_element_type=jnp.floa...]
    ppermute x0 -> x7, starting transfers between devices: none -> 3.06 us  [local(): lax.ppermute(ring[-1], 'sp', [(dev, (dev + 1) % 8) for dev in range(8)])]
  transfers between devices with their start and end apart: 5 -> 12, of which waited for: 4 -> 11; matrix products, arithmetic and copies ran while one was open for 3% -> 3% of each run, Pallas kernels for 0% -> 0%
where the time goes in v1:
time: 284 us; the launch traced here: 283 us
  waiting for transfers between devices  144 us (51%)
  local copies, waits for them, and re-layouts  62.3 us (22%)
  blocking collectives  25.5 us (9%)
  matrix products  21.7 us (8%)
  between operations  13.6 us (5%)
  starting transfers between devices  8.85 us (3%)
  other arithmetic  6.16 us (2%)
    ppermute x7, waiting for transfers between devices, local(): lax.ppermute(ring[-1], 'sp', [(dev, (dev + 1) % 8) for dev in range(8)])  50 us
    unnamed x4, waiting for transfers between devices  33 us
    all_to_all x1, blocking collectives, local(): lax.all_to_all(outgoing, 'sp', split_axis=0, concat_axis=0, tiled=True)  25.5 us
    all_gather x1, waiting for transfers between devices, local(): lax.all_gather(lax.all_to_all(outgoing, 'sp', split_axis=0, concat_axis=0...  22 us
    reduce_scatter x1, waiting for transfers between devices, local(): lax.psum_scatter(jnp.dot(head_out, w_out, preferred_element_type=jnp.floa...  20 us
    all_to_all x1, waiting for transfers between devices, local(): lax.all_to_all(served, 'sp', split_axis=0, concat_axis=0, tiled=True)  19.5 us
    unnamed x82, local copies, waits for them, and re-layouts  19 us
  transfers between devices with their start and end apart: 12, of which 11 were waited for; matrix products, arithmetic and copies ran while one was open for 3% of the time, Pallas kernels for 0%

profile of v1, /device:TPU:0, one launch (start us, length us, event | category | flops | bytes accessed | tf_op | source)
XLA Modules:
  0.0 282.6 jit_solution(382190563640161616)
XLA Ops:
  6.5 1.1 constant_dynamic-slice_fusion.2
  7.7 3.0 %collective-permute-start = (bf16[96,512]{1,0:T(8,128)(2,1)S(1)}, bf16[96,512]{1,0:T(8,128)(2,1)S(1)}, u32[]{:S(2)}, u32[]{:S(2)}) collective-permute-start(bf16[96,512]{1,0:T(8,128)(2,1)S(1)} %fusion.36), channel_id=1, source_target_pairs={{0,4},{4,8},{8,12},{12,16},{16,20},{20,24},{24,28},{28,0},{1,5},{5... | collective-permute-start | bytes 294920 | tf_op jit(solution)/shard_map/ppermute | solution.py:77
  10.7 5.8 %collective-permute-done = bf16[96,512]{1,0:T(8,128)(2,1)S(1)} collective-permute-done((bf16[96,512]{1,0:T(8,128)(2,1)S(1)}, bf16[96,512]{1,0:T(8,128)(2,1)S(1)}, u32[]{:S(2)}, u32[]{:S(2)}) %collective-permute-start) | collective-permute-done | bytes 98336 | tf_op jit(solution)/shard_map/ppermute | solution.py:77
  16.6 7.3 %collective-permute-done.1 = bf16[96,512]{1,0:T(8,128)(2,1)S(1)} collective-permute-done((bf16[96,512]{1,0:T(8,128)(2,1)S(1)}, bf16[96,512]{1,0:T(8,128)(2,1)S(1)}, u32[]{:S(2)}, u32[]{:S(2)}) %collective-permute-start.1) | collective-permute-done | bytes 98336 | tf_op jit(solution)/shard_map/ppermute | solution.py:77
  24.5 7.3 %collective-permute-done.2 = bf16[96,512]{1,0:T(8,128)(2,1)S(1)} collective-permute-done((bf16[96,512]{1,0:T(8,128)(2,1)S(1)}, bf16[96,512]{1,0:T(8,128)(2,1)S(1)}, u32[]{:S(2)}, u32[]{:S(2)}) %collective-permute-start.2) | collective-permute-done | bytes 98336 | tf_op jit(solution)/shard_map/ppermute | solution.py:77
  32.5 7.3 %collective-permute-done.3 = bf16[96,512]{1,0:T(8,128)(2,1)S(1)} collective-permute-done((bf16[96,512]{1,0:T(8,128)(2,1)S(1)}, bf16[96,512]{1,0:T(8,128)(2,1)S(1)}, u32[]{:S(2)}, u32[]{:S(2)}) %collective-permute-start.3) | collective-permute-done | bytes 98336 | tf_op jit(solution)/shard_map/ppermute | solution.py:77
  40.4 7.3 %collective-permute-done.4 = bf16[96,512]{1,0:T(8,128)(2,1)S(1)} collective-permute-done((bf16[96,512]{1,0:T(8,128)(2,1)S(1)}, bf16[96,512]{1,0:T(8,128)(2,1)S(1)}, u32[]{:S(2)}, u32[]{:S(2)}) %collective-permute-start.4) | collective-permute-done | bytes 98336 | tf_op jit(solution)/shard_map/ppermute | solution.py:77
  48.4 8.3 %collective-permute-done.5 = bf16[96,512]{1,0:T(8,128)(2,1)} collective-permute-done((bf16[96,512]{1,0:T(8,128)(2,1)S(1)}, bf16[96,512]{1,0:T(8,128)(2,1)}, u32[]{:S(2)}, u32[]{:S(2)}) %collective-permute-start.5) | collective-permute-done | bytes 98336 | tf_op jit(solution)/shard_map/ppermute | solution.py:77
  56.7 1.0 reshape.102
  57.7 6.6 %collective-permute-done.6 = bf16[96,512]{1,0:T(8,128)(2,1)} collective-permute-done((bf16[96,512]{1,0:T(8,128)(2,1)}, bf16[96,512]{1,0:T(8,128)(2,1)}, u32[]{:S(2)}, u32[]{:S(2)}) %collective-permute-start.6) | collective-permute-done | bytes 98336 | tf_op jit(solution)/shard_map/ppermute | solution.py:77
  71.7 1.3 constant_dynamic-slice_fusion.1
  74.5 1.9 copy.43
  76.4 2.9 %bitcast_reduce_fusion.1 = (f32[192,2,2]{0,1,2:T(2,128)S(1)}, f32[2,768,192,2]{1,2,3,0:T(8,128)}) fusion(bf16[768,2,128,1]{0,2,3,1:T(8,128)(2,1)} %bitcast.120, bf16[192,2,2,128]{3,2,1,0:T(2,128)(2,1)S(1)} %reshape.102), kind=kOutput, calls=%fused_computation.16 | convolution fusion | flops 152173824 | bytes 2952192 | tf_op jit(solution)/shard_map/qhmd,kmd->qhmk/dot_general | solution.py:28
  79.3 1.8 slice.34
  81.1 1.9 reshape.103
  82.9 1.6 bitcast_reduce_fusion
  85.2 1.0 copy-done.1
  86.9 1.6 fusion.18
  88.5 1.5 convolution_add_fusion
  92.5 1.4 fusion.28
  94.7 1.3 copy.53
  98.4 1.3 div.58.clone
  100.2 1.5 convolution_convert_fusion
  102.7 20.0 %reduce-scatter.5.cloned.1.call-done = bf16[48,2048]{1,0:T(8,128)(2,1)} async-done(((bf16[192,2048]{1,0:T(8,128)(2,1)}), bf16[48,2048]{1,0:T(8,128)(2,1)}) %reduce-scatter.5.cloned.1.call-update) | async-done | bytes 196624 | tf_op jit(solution)/shard_map/reduce_scatter | solution.py:90
  122.7 1.1 multiply_reduce_fusion
  123.8 1.0 multiply_convert_fusion.1
  124.9 1.0 broadcast_in_dim.11
  125.9 1.9 reshape.121
  127.7 2.5 scatter_custom_fusion
  130.3 2.1 reshape.105
  132.4 25.5 %all_to_all.10 = bf16[8,18,2048]{2,1,0:T(8,128)(2,1)S(1)} all-to-all(bf16[8,18,2048]{2,1,0:T(8,128)(2,1)} %reshape.105), channel_id=1, replica_groups=mesh['sp'=8,'tp'=4] {'sp'}, dimensions={0} | all-to-all | bytes 1179648 | tf_op jit(solution)/shard_map/all_to_all | solution.py:116
  157.9 1.1 copy.60
  159.3 22.0 %all-gather.2.cloned.1.call-done = bf16[32,18,2048]{2,0,1:T(8,128)(2,1)} async-done(((bf16[8,18,2048]{2,0,1:T(8,128)(2,1)}), bf16[32,18,2048]{2,0,1:T(8,128)(2,1)}) %all-gather.2.cloned.1.call-update) | async-done | bytes 2359312 | tf_op jit(solution)/shard_map/all_gather | solution.py:115
  181.3 4.7 %copy.61 = bf16[32,18,2048]{2,1,0:T(8,128)(2,1)} copy(bf16[32,18,2048]{2,0,1:T(8,128)(2,1)} %all-gather.2.cloned.1.call-done) | data formatting | bytes 4718592 | tf_op jit(solution)/shard_map/all_gather | solution.py:115
  186.0 4.3 %reshape.106 = bf16[576,2048]{1,0:T(8,128)(2,1)} reshape(bf16[32,18,2048]{2,1,0:T(8,128)(2,1)} %copy.61) | data formatting | bytes 4718592 | tf_op jit(solution)/shard_map/reshape | solution.py:121
  190.3 4.7 %fusion.4 = f32[576,768]{1,0:T(8,128)S(1)} fusion(bf16[576,2048]{1,0:T(8,128)(2,1)} %reshape.106, bf16[1,2048,768]{2,1,0:T(8,128)(2,1)} %param.23), kind=kOutput, calls=%fused_computation.6 | convolution fusion | flops 1811939328 | bytes 7274496 | tf_op jit(solution)/shard_map/dot_general | solution.py:122
  195.1 3.0 %multiply_convert_fusion = bf16[576,768]{1,0:T(8,128)(2,1)} fusion(f32[576,768]{1,0:T(8,128)S(1)} %fusion.4, bf16[576,2048]{1,0:T(8,128)(2,1)S(1)} %copy-done.3, bf16[1,2048,768]{2,1,0:T(8,128)(2,1)S(1)} %copy-done.24), kind=kOutput, calls=%fused_computation.21 | convolution fusion | flops 1814593536 | bytes 8159232 | tf_op jit(solution)/shard_map/dot_general | solution.py:123
  198.2 2.3 dot_general.36
  200.4 3.3 %fusion.9 = bf16[18,4,8,2048]{3,2,1,0:T(8,128)(2,1)S(1)} fusion(bf16[1,768,2048]{2,1,0:T(8,128)(2,1)S(1)} %copy-done, bf16[32,18,768]{2,1,0:T(8,128)(2,1)} %dot_general.36), kind=kOutput, calls=%fused_computation.9 | convolution fusion | flops 1813118976 | bytes 6389760 | tf_op jit(solution)/shard_map/dot_general | solution.py:125
  203.7 1.6 copy.79
  205.3 33.0 %reduce-scatter.7.cloned.1.call-done = bf16[8,36864]{1,0:T(8,128)(2,1)} async-done(((bf16[32,36864]{1,0:T(8,128)(2,1)}), bf16[8,36864]{1,0:T(8,128)(2,1)}) %reduce-scatter.7.cloned.1.call-update) | async-done | bytes 589840
  238.3 2.3 copy.63
  240.6 5.5 %all-to-all-start.1 = ((bf16[8,18,2048]{2,1,0:T(8,128)(2,1)}), bf16[8,18,2048]{2,1,0:T(8,128)(2,1)}, u32[]{:S(2)}, u32[]{:S(2)}) async-start(bf16[8,18,2048]{2,1,0:T(8,128)(2,1)} %copy.63), calls=%async_computation.2 | async-start | bytes 1572864 | tf_op jit(solution)/shard_map/all_to_all | solution.py:131
  246.9 19.5 %all-to-all-done.1 = bf16[8,18,2048]{2,1,0:T(8,128)(2,1)} async-done(((bf16[8,18,2048]{2,1,0:T(8,128)(2,1)}), bf16[8,18,2048]{2,1,0:T(8,128)(2,1)}, u32[]{:S(2)}, u32[]{:S(2)}) %all-to-all-start.1) | async-done | bytes 589856 | tf_op jit(solution)/shard_map/all_to_all | solution.py:131
  266.3 2.2 reshape.107
  268.5 3.1 %gather_fusion = bf16[96,2048]{1,0:T(8,128)(2,1)} fusion(bf16[144,2048]{1,0:T(8,128)(2,1)} %reshape.107, s32[1024]{0:T(1024)S(1)} %pad_clamp_fusion), kind=kCustom, calls=%fused_computation | custom fusion | bytes 786816 | tf_op jit(solution)/shard_map/gather | solution.py:134
  271.6 2.0 reshape.108
  273.6 1.5 fusion.42
  (120 shorter events, 21.6 us)
Async XLA Ops:
  6.5 193.9 %copy-start = (bf16[1,768,2048]{2,1,0:T(8,128)(2,1)S(1)}, bf16[1,768,2048]{2,1,0:T(8,128)(2,1)}, u32[]{:S(2)}) copy-start(bf16[1,768,2048]{2,1,0:T(8,128)(2,1)} %param.25) | copy-start | bytes 9437188
  6.5 116.2 %reduce-scatter.5.cloned.1.call-start = ((), (), s32[]{:S(2)}) async-start(), calls=%async_computation.4 | async-start | bytes 983040 | tf_op jit(solution)/shard_map/reduce_scatter | solution.py:90
  7.7 8.9 %collective-permute-start = (bf16[96,512]{1,0:T(8,128)(2,1)S(1)}, bf16[96,512]{1,0:T(8,128)(2,1)S(1)}, u32[]{:S(2)}, u32[]{:S(2)}) collective-permute-start(bf16[96,512]{1,0:T(8,128)(2,1)S(1)} %fusion.36), channel_id=1, source_target_pairs={{0,4},{4,8},{8,12},{12,16},{16,20},{20,24},{24,28},{28,0},{1,5},{5... | collective-permute-start | bytes 294920 | tf_op jit(solution)/shard_map/ppermute | solution.py:77
  16.6 7.3 %collective-permute-start.1 = (bf16[96,512]{1,0:T(8,128)(2,1)S(1)}, bf16[96,512]{1,0:T(8,128)(2,1)S(1)}, u32[]{:S(2)}, u32[]{:S(2)}) collective-permute-start(bf16[96,512]{1,0:T(8,128)(2,1)S(1)} %collective-permute-done), channel_id=1, source_target_pairs={{0,4},{4,8},{8,12},{12,16},{16,20},{20,24},{24,28},{28,0},{1,5},{5... | collective-permute-start | bytes 294920 | tf_op jit(solution)/shard_map/ppermute | solution.py:77
  23.9 0.6 copy-start.9
  24.5 7.3 %collective-permute-start.2 = (bf16[96,512]{1,0:T(8,128)(2,1)S(1)}, bf16[96,512]{1,0:T(8,128)(2,1)S(1)}, u32[]{:S(2)}, u32[]{:S(2)}) collective-permute-start(bf16[96,512]{1,0:T(8,128)(2,1)S(1)} %collective-permute-done.1), channel_id=1, source_target_pairs={{0,4},{4,8},{8,12},{12,16},{16,20},{20,24},{24,28},{28,0},{1,5},{5... | collective-permute-start | bytes 294920 | tf_op jit(solution)/shard_map/ppermute | solution.py:77
  31.8 0.6 copy-start.11
  32.5 7.3 %collective-permute-start.3 = (bf16[96,512]{1,0:T(8,128)(2,1)S(1)}, bf16[96,512]{1,0:T(8,128)(2,1)S(1)}, u32[]{:S(2)}, u32[]{:S(2)}) collective-permute-start(bf16[96,512]{1,0:T(8,128)(2,1)S(1)} %collective-permute-done.2), channel_id=1, source_target_pairs={{0,4},{4,8},{8,12},{12,16},{16,20},{20,24},{24,28},{28,0},{1,5},{5... | collective-permute-start | bytes 294920 | tf_op jit(solution)/shard_map/ppermute | solution.py:77
  39.8 0.6 copy-start.13
  40.4 7.3 %collective-permute-start.4 = (bf16[96,512]{1,0:T(8,128)(2,1)S(1)}, bf16[96,512]{1,0:T(8,128)(2,1)S(1)}, u32[]{:S(2)}, u32[]{:S(2)}) collective-permute-start(bf16[96,512]{1,0:T(8,128)(2,1)S(1)} %collective-permute-done.3), channel_id=1, source_target_pairs={{0,4},{4,8},{8,12},{12,16},{16,20},{20,24},{24,28},{28,0},{1,5},{5... | collective-permute-start | bytes 294920 | tf_op jit(solution)/shard_map/ppermute | solution.py:77
  47.7 0.6 copy-start.15
  48.4 8.3 %collective-permute-start.5 = (bf16[96,512]{1,0:T(8,128)(2,1)S(1)}, bf16[96,512]{1,0:T(8,128)(2,1)}, u32[]{:S(2)}, u32[]{:S(2)}) collective-permute-start(bf16[96,512]{1,0:T(8,128)(2,1)S(1)} %collective-permute-done.4), channel_id=1, source_target_pairs={{0,4},{4,8},{8,12},{12,16},{16,20},{20,24},{24,28},{28,0},{1,5},{5... | collective-permute-start | bytes 294920 | tf_op jit(solution)/shard_map/ppermute | solution.py:77
  56.7 7.6 %collective-permute-start.6 = (bf16[96,512]{1,0:T(8,128)(2,1)}, bf16[96,512]{1,0:T(8,128)(2,1)}, u32[]{:S(2)}, u32[]{:S(2)}) collective-permute-start(bf16[96,512]{1,0:T(8,128)(2,1)} %collective-permute-done.5), channel_id=1, source_target_pairs={{0,4},{4,8},{8,12},{12,16},{16,20},{20,24},{24,28},{28,0},{1,5},{5... | collective-permute-start | bytes 294920 | tf_op jit(solution)/shard_map/ppermute | solution.py:77
  57.7 13.9 %copy-start.16 = (bf16[96,512]{1,0:T(8,128)(2,1)S(1)}, bf16[96,512]{1,0:T(8,128)(2,1)}, u32[]{:S(2)}) copy-start(bf16[96,512]{1,0:T(8,128)(2,1)} %copy-done.15) | copy-start | bytes 294916
  57.7 13.9 %copy-start.14 = (bf16[96,512]{1,0:T(8,128)(2,1)S(1)}, bf16[96,512]{1,0:T(8,128)(2,1)}, u32[]{:S(2)}) copy-start(bf16[96,512]{1,0:T(8,128)(2,1)} %copy-done.13) | copy-start | bytes 294916
  57.7 13.9 %copy-start.12 = (bf16[96,512]{1,0:T(8,128)(2,1)S(1)}, bf16[96,512]{1,0:T(8,128)(2,1)}, u32[]{:S(2)}) copy-start(bf16[96,512]{1,0:T(8,128)(2,1)} %copy-done.11) | copy-start | bytes 294916
  57.7 13.9 %copy-start.10 = (bf16[96,512]{1,0:T(8,128)(2,1)S(1)}, bf16[96,512]{1,0:T(8,128)(2,1)}, u32[]{:S(2)}) copy-start(bf16[96,512]{1,0:T(8,128)(2,1)} %copy-done.9) | copy-start | bytes 294916
  69.7 3.3 %copy-start.21 = (f32[2]{0:T(128)S(1)}, f32[2]{0:T(128)}, u32[]{:S(2)}) copy-start(f32[2]{0:T(128)} %param.16) | copy-start | bytes 28
  69.7 3.3 %copy-start.22 = (f32[256]{0:T(256)S(1)}, f32[256]{0:T(256)}, u32[]{:S(2)}) copy-start(f32[256]{0:T(256)} %param.17) | copy-start | bytes 3076
  71.7 1.9 copy-start.6
  73.0 6.3 %collective-permute-start.7 = (bf16[768,512]{1,0:T(8,128)(2,1)}, bf16[768,512]{1,0:T(8,128)(2,1)}, u32[]{:S(2)}, u32[]{:S(2)}) collective-permute-start(bf16[768,512]{1,0:T(8,128)(2,1)} %constant_dynamic-slice_fusion.1), channel_id=1, source_target_pairs={{0,1},{1,0},{2,3},{3,2},{4,5},{5,4},{6,7},{7,6},{8,9},{9,8},{10,11... | collective-permute-start | bytes 2359304 | tf_op jit(solution)/shard_map/ppermute | solution.py:15
  84.5 1.7 copy-start.1
  90.0 0.9 copy-start.2
  97.1 2.6 copy-start.17
  98.3 1.7 copy-start.7
  98.3 1.7 copy-start.8
  98.3 1.7 copy-start.20
  98.3 1.9 copy-start.25
  100.2 1.6 copy-start.19
  100.2 22.5 %copy-start.4 = (bf16[48,2048]{1,0:T(8,128)(2,1)S(1)}, bf16[48,2048]{1,0:T(8,128)(2,1)}, u32[]{:S(2)}) copy-start(bf16[48,2048]{1,0:T(8,128)(2,1)} %param.19) | copy-start | bytes 589828
  100.2 23.6 %copy-start.18 = (f32[2048]{0:T(1024)S(1)}, f32[2048]{0:T(1024)}, u32[]{:S(2)}) copy-start(f32[2048]{0:T(1024)} %param.20) | copy-start | bytes 24580
  101.8 79.5 %all-gather.2.cloned.1.call-start = ((), (), s32[]{:S(2)}) async-start(), calls=%async_computation.5 | async-start | bytes 2949120 | tf_op jit(solution)/shard_map/all_gather | solution.py:115
  159.0 79.2 %reduce-scatter.7.cloned.1.call-start = ((), (), s32[]{:S(2)}) async-start(), calls=%async_computation.6 | async-start | bytes 2949120
  190.3 4.7 %copy-start.3 = (bf16[576,2048]{1,0:T(8,128)(2,1)S(1)}, bf16[576,2048]{1,0:T(8,128)(2,1)}, u32[]{:S(2)}) copy-start(bf16[576,2048]{1,0:T(8,128)(2,1)} %reshape.106) | copy-start | bytes 7077892
  190.3 4.8 %copy-start.24 = (bf16[1,2048,768]{2,1,0:T(8,128)(2,1)S(1)}, bf16[1,2048,768]{2,1,0:T(8,128)(2,1)}, u32[]{:S(2)}) copy-start(bf16[1,2048,768]{2,1,0:T(8,128)(2,1)} %param.24) | copy-start | bytes 9437188
  205.3 40.8 %copy-start.23 = (f32[48,2]{0,1:T(2,128)S(1)}, f32[48,2]{0,1:T(2,128)}, u32[]{:S(2)}) copy-start(f32[48,2]{0,1:T(2,128)} %param.22) | copy-start | bytes 1156
  240.6 25.7 %all-to-all-start.1 = ((bf16[8,18,2048]{2,1,0:T(8,128)(2,1)}), bf16[8,18,2048]{2,1,0:T(8,128)(2,1)}, u32[]{:S(2)}, u32[]{:S(2)}) async-start(bf16[8,18,2048]{2,1,0:T(8,128)(2,1)} %copy.63), calls=%async_computation.2 | async-start | bytes 1572864 | tf_op jit(solution)/shard_map/all_to_all | solution.py:131
  271.6 3.6 %copy-start.5 = (bf16[48,2048]{1,0:T(8,128)(2,1)S(1)}, bf16[48,2048]{1,0:T(8,128)(2,1)}, u32[]{:S(2)}) copy-start(bf16[48,2048]{1,0:T(8,128)(2,1)} %reduce-scatter.5.cloned.1.call-done) | copy-start | bytes 589828
Sparse Core Ops, SparseCore 0:
  101.9 20.7 reduce-scatter.4
  159.2 22.1 all-gather.1
  205.4 32.8 reduce-scatter.6
